TPU v7x, 32 devices: a whole 2x2x4 slice. The times are simulated.
32 devices in a mesh: fs: 16 (over z, y, x), tp: 2 (over core).
Axes of the slice: x: 2, y: 2, z: 4, core: 2. Of those that a mesh axis runs over, the one named last changes fastest.
Arguments:
- tokens: bfloat16 [2, 256, 2048], P('tp'), may hold values from -6 to 6
- gain_first: float32 [2048], P('fs'), may hold values from 0.1 to 1.9
- gate_first: float32 [2048, 5632], P('fs', 'tp'), may hold values from -0.125 to 0.125
- up_first: float32 [2048, 5632], P('fs', 'tp'), may hold values from -0.125 to 0.125
- down_first: float32 [2048, 5632], P('fs', 'tp'), may hold values from -0.3125 to 0.3125
- gain_second: float32 [2048], P('fs'), may hold values from 0.1 to 1.9
- gate_second: float32 [2048, 5632], P('fs', 'tp'), may hold values from -0.125 to 0.125
- up_second: float32 [2048, 5632], P('fs', 'tp'), may hold values from -0.125 to 0.125
- down_second: float32 [2048, 5632], P('fs', 'tp'), may hold values from -0.3125 to 0.3125
Outputs:
- mixed: bfloat16 [2, 256, 2048], P('tp', 'fs')
- served_gate_first: bfloat16 [2, 2816, 2048], P(None, 'fs')
- served_up_first: bfloat16 [2, 2816, 2048], P(None, 'fs')
- served_down_first: bfloat16 [2, 2816, 2048], P(None, 'fs')
- served_gate_second: bfloat16 [2, 2816, 2048], P(None, 'fs')
- served_up_second: bfloat16 [2, 2816, 2048], P(None, 'fs')
- served_down_second: bfloat16 [2, 2816, 2048], P(None, 'fs')
All inputs are finite; a program needn't handle non-finite values.
Results may differ from a plain program's by a relative error of at most 0.013.
Values may be sent and summed in bfloat16 or wider, within the bound.
A program may use at most 64 MiB of HBM per device.

v0:
```python
import jax
import jax.numpy as jnp
from jax import lax
from jax.sharding import PartitionSpec as P


def normalize(values):
    wide = values.astype(jnp.float32)
    scale = lax.rsqrt(jnp.mean(wide * wide, axis=-1, keepdims=True) + 1e-06)
    return (wide * scale).astype(jnp.bfloat16)


def folded(weight, gain):
    return (weight * gain[:, None]).astype(jnp.bfloat16).T


def relayout(gate_part, up_part, down_part):
    gate_cut, up_cut, down_cut = (
        lax.all_to_all(gate_part, "fs", split_axis=0, concat_axis=1, tiled=True),
        lax.all_to_all(up_part, "fs", split_axis=0, concat_axis=1, tiled=True),
        lax.all_to_all(down_part, "fs", split_axis=0, concat_axis=1, tiled=True),
    )
    return (
        lax.all_gather(gate_cut[None], "tp", axis=0, tiled=True),
        lax.all_gather(up_cut[None], "tp", axis=0, tiled=True),
        lax.all_gather(down_cut[None], "tp", axis=0, tiled=True),
    )


def hidden_of(normed, gate_served, up_served):
    gate_flat = gate_served.reshape(-1, gate_served.shape[2])
    up_flat = up_served.reshape(-1, up_served.shape[2])
    gate_act = jnp.einsum("rd,hd->rh", normed, gate_flat, preferred_element_type=jnp.float32)
    up_act = jnp.einsum("rd,hd->rh", normed, up_flat, preferred_element_type=jnp.float32)
    return (jax.nn.silu(gate_act) * up_act).astype(jnp.bfloat16)


def projector(hidden, down_flat):
    return jnp.dot(hidden, down_flat, preferred_element_type=jnp.float32)


def shards(
    tokens,
    gain_first,
    gate_first,
    up_first,
    down_first,
    gain_second,
    gate_second,
    up_second,
    down_second,
):
    gate_one, up_one, down_one = relayout(
        folded(gate_first, gain_first),
        folded(up_first, gain_first),
        down_first.astype(jnp.bfloat16).T,
    )
    gate_two, up_two, down_two = relayout(
        folded(gate_second, gain_second),
        folded(up_second, gain_second),
        down_second.astype(jnp.bfloat16).T,
    )
    rows = tokens[0]
    keep = rows.shape[0] // lax.axis_size("fs")
    offset = lax.axis_index("fs") * keep
    hidden_first = hidden_of(normalize(rows), gate_one, up_one)
    down_flat_one = down_one.reshape(-1, down_one.shape[2])
    partial_value = jnp.dot(hidden_first, down_flat_one, preferred_element_type=jnp.float32)
    branch = lax.psum(partial_value, "fs")
    whole_middle = (rows.astype(jnp.float32) + 0.5 * branch).astype(jnp.bfloat16)
    hidden_second = hidden_of(normalize(whole_middle), gate_two, up_two)
    middle = lax.dynamic_slice_in_dim(whole_middle, offset, keep, 0)
    down_flat_two = down_two.reshape(-1, down_two.shape[2])
    branch_two = lax.psum_scatter(
        projector(hidden_second, down_flat_two), "fs", scatter_dimension=0, tiled=True
    )
    mixed = (middle.astype(jnp.float32) + 0.5 * branch_two).astype(jnp.bfloat16)[None]
    return (mixed, gate_one, up_one, down_one, gate_two, up_two, down_two)


def solution(mesh):
    return jax.shard_map(
        shards,
        mesh=mesh,
        in_specs=(
            P("tp", None, None),
            P("fs"),
            P("fs", "tp"),
            P("fs", "tp"),
            P("fs", "tp"),
            P("fs"),
            P("fs", "tp"),
            P("fs", "tp"),
            P("fs", "tp"),
        ),
        out_specs=(
            P("tp", "fs", None),
            P(None, "fs", None),
            P(None, "fs", None),
            P(None, "fs", None),
            P(None, "fs", None),
            P(None, "fs", None),
            P(None, "fs", None),
        ),
        check_vma=False,
    )
```

profile of v0, /device:TPU:0, one launch (start us, length us, event | category | flops | bytes accessed | tf_op | source)
XLA Modules:
  0.0 395.1 jit_solution(5311903597791260053)
XLA Ops:
  7.2 0.0 all-gather.7.cloned.1.call-start
  7.2 1.8 copy.40
  9.0 1.8 copy.42
  10.8 1.1 multiply_convert_fusion.3
  11.9 28.1 %all_to_all.96 = bf16[16,176,128]{2,1,0:T(8,128)(2,1)S(1)} all-to-all(bf16[16,176,128]{2,1,0:T(8,128)(2,1)S(1)} %bitcast.56), channel_id=1, replica_groups=mesh['fs'=16,'tp'=2] {'fs'}, dimensions={0} | all-to-all | bytes 1441792 | tf_op jit(solution)/shard_map/all_to_all | solution.py:19
  40.1 0.2 copy.41
  40.3 1.2 broadcast_in_dim.27
  41.4 0.0 all-gather.9.cloned.1.call-start
  41.5 22.3 %all_to_all.97 = bf16[16,176,128]{2,1,0:T(8,128)(2,1)S(1)} all-to-all(bf16[16,176,128]{2,1,0:T(8,128)(2,1)S(1)} %bitcast.54), channel_id=1, replica_groups=mesh['fs'=16,'tp'=2] {'fs'}, dimensions={0} | all-to-all | bytes 1441792 | tf_op jit(solution)/shard_map/all_to_all | solution.py:20
  63.8 0.2 copy.43
  64.0 1.2 broadcast_in_dim.28
  65.2 0.0 all-gather.11.cloned.1.call-start
  65.3 0.4 copy-done.3
  65.7 0.4 copy.44
  66.0 22.3 %all_to_all.98 = bf16[16,176,128]{2,1,0:T(8,128)(2,1)S(1)} all-to-all(bf16[16,176,128]{2,1,0:T(8,128)(2,1)S(1)} %bitcast.64), channel_id=1, replica_groups=mesh['fs'=16,'tp'=2] {'fs'}, dimensions={0} | all-to-all | bytes 1441792 | tf_op jit(solution)/shard_map/all_to_all | solution.py:21
  88.3 0.2 copy.45
  88.5 1.2 broadcast_in_dim.29
  89.7 0.0 all-reduce.2.cloned.1.call-start
  89.8 0.4 copy-done.4
  90.1 0.4 copy.46
  90.6 1.8 copy.48
  92.4 1.6 fusion.4
  94.0 0.0 all-gather.7.cloned.1.call-done
  94.0 2.5 fusion.14
  96.5 0.0 all-gather.9.cloned.1.call-done
  96.5 0.6 all-gather.11.cloned.1.call-done
  97.1 5.5 %fusion.10 = f32[256,2048]{1,0:T(8,128)} fusion(bf16[352,2048]{1,0:T(8,128)(2,1)} %bitcast.68, bf16[352,2048]{1,0:T(8,128)(2,1)} %bitcast.67, bf16[1,256,2048]{2,1,0:T(8,128)(2,1)} %param.9, f32[256]{0:T(256)S(1)} %add_rsqrt_fusion.1, f32[256,352]{0,1:T(8,128)S(1)} %fusion.14), kind=kOutput, calls=%fused_computation.20 | convolution fusion | flops 740311040 | bytes 6390784 | tf_op jit(solution)/shard_map/dot_general | solution.py:68
  102.6 0.0 all-gather.13.cloned.1.call-start
  102.7 0.6 copy-done.13
  103.3 1.1 multiply_convert_fusion.1
  104.3 41.4 %all_to_all.99 = bf16[16,176,128]{2,1,0:T(8,128)(2,1)S(1)} all-to-all(bf16[16,176,128]{2,1,0:T(8,128)(2,1)S(1)} %bitcast.57), channel_id=1, replica_groups=mesh['fs'=16,'tp'=2] {'fs'}, dimensions={0} | all-to-all | bytes 1441792 | tf_op jit(solution)/shard_map/all_to_all | solution.py:19
  145.7 0.2 copy.47
  145.9 1.2 broadcast_in_dim.30
  147.1 0.0 all-gather.15.cloned.1.call-start
  147.2 26.7 %all_to_all.100 = bf16[16,176,128]{2,1,0:T(8,128)(2,1)S(1)} all-to-all(bf16[16,176,128]{2,1,0:T(8,128)(2,1)S(1)} %bitcast.55), channel_id=1, replica_groups=mesh['fs'=16,'tp'=2] {'fs'}, dimensions={0} | all-to-all | bytes 1441792 | tf_op jit(solution)/shard_map/all_to_all | solution.py:20
  173.9 0.2 copy.49
  174.1 1.2 broadcast_in_dim.31
  175.3 0.0 all-gather.17.cloned.1.call-start
  175.3 0.4 copy-done.5
  175.7 0.3 copy.50
  176.0 23.5 %all_to_all.101 = bf16[16,176,128]{2,1,0:T(8,128)(2,1)S(1)} all-to-all(bf16[16,176,128]{2,1,0:T(8,128)(2,1)S(1)} %bitcast.65), channel_id=1, replica_groups=mesh['fs'=16,'tp'=2] {'fs'}, dimensions={0} | all-to-all | bytes 1441792 | tf_op jit(solution)/shard_map/all_to_all | solution.py:21
  199.5 0.2 copy.51
  199.7 1.2 broadcast_in_dim.32
  200.9 0.2 reduce-scatter.2.cloned.1.call-start
  201.2 50.3 %all-reduce.2.cloned.1.call-done = f32[256,2048]{1,0:T(8,128)} async-done(((f32[256,2048]{1,0:T(8,128)}), f32[256,2048]{1,0:T(8,128)}) %all-reduce.2.cloned.1.call-update) | async-done | bytes 2097168 | tf_op jit(solution)/shard_map/psum | solution.py:69
  251.4 2.1 fusion.2
  253.6 8.7 %all-gather.13.cloned.1.call-done = bf16[2,176,2048]{2,1,0:T(8,128)(2,1)} async-done(((bf16[1,176,2048]{2,1,0:T(8,128)(2,1)}), bf16[2,176,2048]{2,1,0:T(8,128)(2,1)}) %all-gather.13.cloned.1.call-update) | async-done | bytes 1441808 | tf_op jit(solution)/shard_map/all_gather | solution.py:24
  262.3 2.0 fusion.18
  264.3 10.8 %all-gather.15.cloned.1.call-done = bf16[2,176,2048]{2,1,0:T(8,128)(2,1)} async-done(((bf16[1,176,2048]{2,1,0:T(8,128)(2,1)}), bf16[2,176,2048]{2,1,0:T(8,128)(2,1)}) %all-gather.15.cloned.1.call-update) | async-done | bytes 1441808 | tf_op jit(solution)/shard_map/all_gather | solution.py:25
  275.1 12.9 %all-gather.17.cloned.1.call-done = bf16[2,176,2048]{2,1,0:T(8,128)(2,1)} async-done(((bf16[1,176,2048]{2,1,0:T(8,128)(2,1)}), bf16[2,176,2048]{2,1,0:T(8,128)(2,1)}) %all-gather.17.cloned.1.call-update) | async-done | bytes 1441808 | tf_op jit(solution)/shard_map/all_gather | solution.py:26
  288.0 5.2 %fusion.9 = f32[256,2048]{1,0:T(8,128)} fusion(bf16[352,2048]{1,0:T(8,128)(2,1)} %bitcast.71, bf16[352,2048]{1,0:T(8,128)(2,1)} %bitcast.70, bf16[256,2048]{1,0:T(8,128)(2,1)S(1)} %get-tuple-element.8, f32[256]{0:T(256)S(1)} %add_rsqrt_fusion, f32[256,352]{0,1:T(8,128)S(1)} %fusion.18), kind=kOutput, calls=%fused_computation.19 | convolution fusion | flops 740311040 | bytes 6390784 | tf_op jit(solution)/shard_map/dot_general | solution.py:39
  293.3 82.9 %reduce-scatter.2.cloned.1.call-done = f32[16,2048]{1,0:T(8,128)} async-done(((f32[256,2048]{1,0:T(8,128)}), f32[16,2048]{1,0:T(8,128)}) %reduce-scatter.2.cloned.1.call-update) | async-done | bytes 131088 | tf_op jit(solution)/shard_map/reduce_scatter | solution.py:74
  376.2 1.6 fusion.32
  377.7 1.1 copy.59
  378.8 0.8 copy-done.7
  379.6 1.1 copy.60
  380.7 0.8 copy-done.8
  381.5 1.1 copy.61
  382.6 0.8 copy-done.9
  383.4 1.1 copy.62
  384.5 0.8 copy-done.10
  385.3 1.1 copy.63
  386.4 0.8 copy-done.11
  387.1 1.1 copy.64
  (29 shorter events, 0.2 us)
Async XLA Ops:
  7.2 86.8 %all-gather.7.cloned.1.call-start = ((), (), s32[]{:S(2)}) async-start(), calls=%async_computation.7 | async-start | bytes 2162688 | tf_op jit(solution)/shard_map/all_gather | solution.py:24
  9.0 1.8 copy-start.12
  40.2 1.3 copy-start.1
  41.4 55.1 %all-gather.9.cloned.1.call-start = ((), (), s32[]{:S(2)}) async-start(), calls=%async_computation.8 | async-start | bytes 2162688 | tf_op jit(solution)/shard_map/all_gather | solution.py:25
  64.0 1.6 copy-start.3
  65.2 31.9 %all-gather.11.cloned.1.call-start = ((), (), s32[]{:S(2)}) async-start(), calls=%async_computation.9 | async-start | bytes 2162688 | tf_op jit(solution)/shard_map/all_gather | solution.py:26
  88.5 1.6 copy-start.4
  89.7 161.7 %all-reduce.2.cloned.1.call-start = ((), (), s32[]{:S(2)}) async-start(), calls=%async_computation.10 | async-start | bytes 4194304 | tf_op jit(solution)/shard_map/psum | solution.py:69
  102.6 0.7 copy-start.13
  102.6 159.6 %all-gather.13.cloned.1.call-start = ((), (), s32[]{:S(2)}) async-start(), calls=%async_computation.11 | async-start | bytes 2162688 | tf_op jit(solution)/shard_map/all_gather | solution.py:24
  145.9 1.3 copy-start.2
  147.1 127.9 %all-gather.15.cloned.1.call-start = ((), (), s32[]{:S(2)}) async-start(), calls=%async_computation.12 | async-start | bytes 2162688 | tf_op jit(solution)/shard_map/all_gather | solution.py:25
  174.1 1.6 copy-start.5
  175.3 112.7 %all-gather.17.cloned.1.call-start = ((), (), s32[]{:S(2)}) async-start(), calls=%async_computation.13 | async-start | bytes 2162688 | tf_op jit(solution)/shard_map/all_gather | solution.py:26
  199.7 51.7 %copy-start = (bf16[1,256,2048]{2,1,0:T(8,128)(2,1)S(1)}, bf16[1,256,2048]{2,1,0:T(8,128)(2,1)}, u32[]{:S(2)}) copy-start(bf16[1,256,2048]{2,1,0:T(8,128)(2,1)} %param.9) | copy-start | bytes 3145732
  200.9 175.2 %reduce-scatter.2.cloned.1.call-start = ((), (), s32[]{:S(2)}) async-start(), calls=%async_computation.14 | async-start | bytes 2228224 | tf_op jit(solution)/shard_map/reduce_scatter | solution.py:74
  293.2 84.5 %copy-start.6 = (bf16[2,176,2048]{2,1,0:T(8,128)(2,1)S(1)}, bf16[2,176,2048]{2,1,0:T(8,128)(2,1)}, u32[]{:S(2)}) copy-start(bf16[2,176,2048]{2,1,0:T(8,128)(2,1)} %all-gather.7.cloned.1.call-done) | copy-start | bytes 4325380
  377.7 1.9 copy-start.7
  379.6 1.9 copy-start.8
  381.5 1.9 copy-start.9
  383.4 1.9 copy-start.10
  385.3 1.9 copy-start.11
Sparse Core Ops, SparseCore 0:
  41.6 7.2 all-gather.6
  65.3 7.2 all-gather.8
  89.8 7.2 all-gather.10
  102.8 148.6 all-reduce.1
  253.4 8.8 all-gather.12
  264.3 10.7 all-gather.14
  277.2 10.7 all-gather.16
  293.4 82.7 reduce-scatter.1
where the time goes:
time: 396 us; the launch traced here: 395 us
  waiting for transfers between devices  166 us (42%)
  blocking collectives  164 us (41%)
  local copies, waits for them, and re-layouts  26.9 us (7%)
  matrix products  15.3 us (4%)
  between operations  14.3 us (4%)
  other arithmetic  7.42 us (2%)
    reduce_scatter x1, waiting for transfers between devices, shards(): lax.psum_scatter(projector(hidden_second, down_flat_two), 'fs', scatter_d...  82.9 us
    all_to_all x2, blocking collectives, relayout(): lax.all_to_all(gate_part, 'fs', split_axis=0, concat_axis=1, tiled=True)  69.5 us
    psum x1, waiting for transfers between devices, shards(): branch = lax.psum(partial_value, 'fs')  50.3 us
    all_to_all x2, blocking collectives, relayout(): lax.all_to_all(up_part, 'fs', split_axis=0, concat_axis=1, tiled=True)  49 us
    all_to_all x2, blocking collectives, relayout(): lax.all_to_all(down_part, 'fs', split_axis=0, concat_axis=1, tiled=True)  45.8 us
    unnamed x40, local copies, waits for them, and re-layouts  18.8 us
    all_gather x2, waiting for transfers between devices, relayout(): lax.all_gather(down_cut[None], 'tp', axis=0, tiled=True)  13.5 us
    all_gather x2, waiting for transfers between devices, relayout(): lax.all_gather(up_cut[None], 'tp', axis=0, tiled=True)  10.8 us
  transfers between devices with their start and end apart: 8, of which 6 were waited for; matrix products, arithmetic and copies ran while one was open for 5% of the time, Pallas kernels for 0%

commit v1 on v0

--- a/solution.py
+++ b/solution.py
@@ -2,6 +2,11 @@
 import jax.numpy as jnp
 from jax import lax
 from jax.sharding import PartitionSpec as P
+
+
+def finish_pools_over_axis(vec, a_name):
+    finding = jax.lax.all_gather(vec, a_name).sum(axis=0)
+    return finding
 
 
 def normalize(values):
@@ -66,7 +71,7 @@
     hidden_first = hidden_of(normalize(rows), gate_one, up_one)
     down_flat_one = down_one.reshape(-1, down_one.shape[2])
     partial_value = jnp.dot(hidden_first, down_flat_one, preferred_element_type=jnp.float32)
-    branch = lax.psum(partial_value, "fs")
+    branch = finish_pools_over_axis(partial_value, a_name="fs")
     whole_middle = (rows.astype(jnp.float32) + 0.5 * branch).astype(jnp.bfloat16)
     hidden_second = hidden_of(normalize(whole_middle), gate_two, up_two)
     middle = lax.dynamic_slice_in_dim(whole_middle, offset, keep, 0)

time: 396 us -> 641 us (1.62)
  waiting for transfers between devices: 166 us -> 365 us
  blocking collectives: 164 us -> 198 us
  other arithmetic: 7.42 us -> 19.6 us
    all_gather x0 -> x1, waiting for transfers between devices: none -> 259 us  [finish_pools_over_axis(): finding = jax.lax.all_gather(vec, a_name).sum(axis=0)]
    psum x1 -> x0, waiting for transfers between devices: 50.3 us -> none  [shards(): branch = lax.psum(partial_value, 'fs')]
    all_to_all x2, blocking collectives: 45.8 us -> 63.9 us  [relayout(): lax.all_to_all(down_part, 'fs', split_axis=0, concat_axis=1, tiled=True)]
    reduce_sum x0 -> x1, other arithmetic: none -> 12.4 us  [finish_pools_over_axis(): finding = jax.lax.all_gather(vec, a_name).sum(axis=0)]
    all_to_all x2, blocking collectives: 49 us -> 60.6 us  [relayout(): lax.all_to_all(up_part, 'fs', split_axis=0, concat_axis=1, tiled=True)]
    all_gather x2, waiting for transfers between devices: 8.75 us -> 0.02 us  [relayout(): lax.all_gather(gate_cut[None], 'tp', axis=0, tiled=True)]
    unnamed x40 -> x38, local copies, waits for them, and re-layouts: 18.8 us -> 20.3 us
  transfers between devices with their start and end apart: 8 -> 8, of which waited for: 6 -> 5; matrix products, arithmetic and copies ran while one was open for 5% -> 5% of each run, Pallas kernels for 0% -> 0%
where the time goes in v1:
time: 641 us
  waiting for transfers between devices  365 us (57%)
  blocking collectives  198 us (31%)
  local copies, waits for them, and re-layouts  28.4 us (4%)
  other arithmetic  19.6 us (3%)
  matrix products  14.7 us (2%)
  between operations  14.3 us (2%)
    all_gather x1, waiting for transfers between devices, finish_pools_over_axis(): finding = jax.lax.all_gather(vec, a_name).sum(axis=0)  259 us
    reduce_scatter x1, waiting for transfers between devices, shards(): lax.psum_scatter(projector(hidden_second, down_flat_two), 'fs', scatter_d...  82.7 us
    all_to_all x2, blocking collectives, relayout(): lax.all_to_all(gate_part, 'fs', split_axis=0, concat_axis=1, tiled=True)  73.2 us
    all_to_all x2, blocking collectives, relayout(): lax.all_to_all(down_part, 'fs', split_axis=0, concat_axis=1, tiled=True)  63.9 us
    all_to_all x2, blocking collectives, relayout(): lax.all_to_all(up_part, 'fs', split_axis=0, concat_axis=1, tiled=True)  60.6 us
    unnamed x38, local copies, waits for them, and re-layouts  20.3 us
    all_gather x2, waiting for transfers between devices, relayout(): lax.all_gather(down_cut[None], 'tp', axis=0, tiled=True)  17.9 us
  transfers between devices with their start and end apart: 8, of which 5 were waited for; matrix products, arithmetic and copies ran while one was open for 5% of the time, Pallas kernels for 0%

profile of v1, /device:TPU:0, one launch (start us, length us, event | category | flops | bytes accessed | tf_op | source)
XLA Modules:
  0.0 640.5 jit_solution(450842090219323141)
XLA Ops:
  7.2 0.0 all-gather.9.cloned.1.call-start
  7.2 1.8 copy.40
  9.0 1.8 copy.42
  10.8 1.1 multiply_convert_fusion.4
  11.9 28.1 %all_to_all.96 = bf16[16,176,128]{2,1,0:T(8,128)(2,1)S(1)} all-to-all(bf16[16,176,128]{2,1,0:T(8,128)(2,1)S(1)} %bitcast.69), channel_id=1, replica_groups=mesh['fs'=16,'tp'=2] {'fs'}, dimensions={0} | all-to-all | bytes 1441792 | tf_op jit(solution)/shard_map/all_to_all | solution.py:24
  40.1 0.2 copy.41
  40.3 1.2 broadcast_in_dim.27
  41.4 0.0 all-gather.9.cloned.1.call-update
  41.4 0.0 all-gather.11.cloned.1.call-start
  41.5 22.3 %all_to_all.97 = bf16[16,176,128]{2,1,0:T(8,128)(2,1)S(1)} all-to-all(bf16[16,176,128]{2,1,0:T(8,128)(2,1)S(1)} %bitcast.67), channel_id=1, replica_groups=mesh['fs'=16,'tp'=2] {'fs'}, dimensions={0} | all-to-all | bytes 1441792 | tf_op jit(solution)/shard_map/all_to_all | solution.py:25
  63.8 0.2 copy.43
  64.0 1.2 broadcast_in_dim.28
  65.2 0.0 all-gather.13.cloned.1.call-start
  65.3 0.4 copy-done.6
  65.7 0.4 copy.44
  66.0 22.3 %all_to_all.98 = bf16[16,176,128]{2,1,0:T(8,128)(2,1)S(1)} all-to-all(bf16[16,176,128]{2,1,0:T(8,128)(2,1)S(1)} %bitcast.77), channel_id=1, replica_groups=mesh['fs'=16,'tp'=2] {'fs'}, dimensions={0} | all-to-all | bytes 1441792 | tf_op jit(solution)/shard_map/all_to_all | solution.py:26
  88.3 0.2 copy.45
  88.5 1.2 broadcast_in_dim.29
  89.7 0.0 all-gather.21.cloned.1.call-start
  89.8 0.3 fusion.2
  90.1 0.0 all-gather.9.cloned.1.call-done
  90.1 2.0 fusion.14
  92.1 0.0 all-gather.11.cloned.1.call-done
  92.1 4.9 all-gather.13.cloned.1.call-done
  97.1 5.2 fusion.9
  102.3 0.0 all-gather.15.cloned.1.call-start
  102.4 1.8 copy.46
  104.2 2.9 copy.48
  107.1 1.6 multiply_convert_fusion.2
  108.7 45.1 %all_to_all.99 = bf16[16,176,128]{2,1,0:T(8,128)(2,1)S(1)} all-to-all(bf16[16,176,128]{2,1,0:T(8,128)(2,1)S(1)} %bitcast.70), channel_id=1, replica_groups=mesh['fs'=16,'tp'=2] {'fs'}, dimensions={0} | all-to-all | bytes 1441792 | tf_op jit(solution)/shard_map/all_to_all | solution.py:24
  153.7 0.2 copy.47
  153.9 1.2 broadcast_in_dim.30
  155.1 0.0 all-gather.17.cloned.1.call-start
  155.1 38.3 %all_to_all.100 = bf16[16,176,128]{2,1,0:T(8,128)(2,1)S(1)} all-to-all(bf16[16,176,128]{2,1,0:T(8,128)(2,1)S(1)} %bitcast.68), channel_id=1, replica_groups=mesh['fs'=16,'tp'=2] {'fs'}, dimensions={0} | all-to-all | bytes 1441792 | tf_op jit(solution)/shard_map/all_to_all | solution.py:25
  193.4 0.2 copy.49
  193.6 1.2 broadcast_in_dim.31
  194.8 0.0 all-gather.19.cloned.1.call-start
  194.8 0.4 copy-done.7
  195.2 0.3 copy.50
  195.6 41.6 %all_to_all.101 = bf16[16,176,128]{2,1,0:T(8,128)(2,1)S(1)} all-to-all(bf16[16,176,128]{2,1,0:T(8,128)(2,1)S(1)} %bitcast.78), channel_id=1, replica_groups=mesh['fs'=16,'tp'=2] {'fs'}, dimensions={0} | all-to-all | bytes 1441792 | tf_op jit(solution)/shard_map/all_to_all | solution.py:26
  237.1 0.2 copy.51
  237.3 1.2 broadcast_in_dim.32
  238.5 0.2 reduce-scatter.2.cloned.1.call-start
  238.7 259.4 %all-gather.21.cloned.1.call-done = f32[4096,2048]{1,0:T(8,128)} async-done(((f32[256,2048]{1,0:T(8,128)}), f32[4096,2048]{1,0:T(8,128)}) %all-gather.21.cloned.1.call-update) | async-done | bytes 33554448 | tf_op jit(solution)/shard_map/all_gather | solution.py:8
  498.2 12.4 %reduce_sum.28 = f32[256,2048]{1,0:T(8,128)S(1)} reduce(f32[16,256,2048]{2,1,0:T(8,128)} %bitcast.63, f32[]{:T(128)} %constant.10.clone.1), dimensions={0}, to_apply=%region_1.2 | reduce | flops 7864320 | bytes 35651588 | tf_op jit(solution)/shard_map/reduce_sum | solution.py:8
  510.5 1.5 multiply_reduce_fusion
  512.0 1.3 fusion.10
  513.3 2.3 fusion.32
  515.6 5.1 all-gather.17.cloned.1.call-done
  520.7 12.9 %all-gather.19.cloned.1.call-done = bf16[2,176,2048]{2,1,0:T(8,128)(2,1)} async-done(((bf16[1,176,2048]{2,1,0:T(8,128)(2,1)}), bf16[2,176,2048]{2,1,0:T(8,128)(2,1)}) %all-gather.19.cloned.1.call-update) | async-done | bytes 1441808 | tf_op jit(solution)/shard_map/all_gather | solution.py:31
  533.7 5.2 fusion.8
  538.9 82.7 %reduce-scatter.2.cloned.1.call-done = f32[16,2048]{1,0:T(8,128)} async-done(((f32[256,2048]{1,0:T(8,128)}), f32[16,2048]{1,0:T(8,128)}) %reduce-scatter.2.cloned.1.call-update) | async-done | bytes 131088 | tf_op jit(solution)/shard_map/reduce_scatter | solution.py:79
  621.6 1.6 fusion.28
  623.2 1.1 copy.58
  624.3 0.8 copy-done.9
  625.0 1.1 copy.59
  626.1 0.8 copy-done.10
  626.9 1.1 copy.60
  628.0 0.8 copy-done.2
  628.8 1.1 copy.61
  629.9 0.8 copy-done.3
  630.7 1.1 copy.62
  631.8 0.8 copy-done.4
  632.6 1.1 copy.63
  (29 shorter events, 0.2 us)
Async XLA Ops:
  7.2 82.9 %all-gather.9.cloned.1.call-start = ((), (), s32[]{:S(2)}) async-start(), calls=%async_computation.7 | async-start | bytes 2162688 | tf_op jit(solution)/shard_map/all_gather | solution.py:29
  9.0 1.8 copy-start.11
  40.2 1.3 copy-start.5
  41.4 50.7 %all-gather.11.cloned.1.call-start = ((), (), s32[]{:S(2)}) async-start(), calls=%async_computation.8 | async-start | bytes 2162688 | tf_op jit(solution)/shard_map/all_gather | solution.py:30
  64.0 1.6 copy-start.6
  65.2 31.9 %all-gather.13.cloned.1.call-start = ((), (), s32[]{:S(2)}) async-start(), calls=%async_computation.9 | async-start | bytes 2162688 | tf_op jit(solution)/shard_map/all_gather | solution.py:31
  88.5 1.3 copy-start
  89.7 408.4 %all-gather.21.cloned.1.call-start = ((), (), s32[]{:S(2)}) async-start(), calls=%async_computation.14 | async-start | bytes 35651584 | tf_op jit(solution)/shard_map/all_gather | solution.py:8
  102.3 411.0 %all-gather.15.cloned.1.call-start = ((), (), s32[]{:S(2)}) async-start(), calls=%async_computation.10 | async-start | bytes 2162688 | tf_op jit(solution)/shard_map/all_gather | solution.py:29
  104.2 2.9 copy-start.12
  155.1 365.6 %all-gather.17.cloned.1.call-start = ((), (), s32[]{:S(2)}) async-start(), calls=%async_computation.11 | async-start | bytes 2162688 | tf_op jit(solution)/shard_map/all_gather | solution.py:30
  193.6 1.6 copy-start.7
  194.8 338.9 %all-gather.19.cloned.1.call-start = ((), (), s32[]{:S(2)}) async-start(), calls=%async_computation.12 | async-start | bytes 2162688 | tf_op jit(solution)/shard_map/all_gather | solution.py:31
  238.5 383.1 %reduce-scatter.2.cloned.1.call-start = ((), (), s32[]{:S(2)}) async-start(), calls=%async_computation.13 | async-start | bytes 2228224 | tf_op jit(solution)/shard_map/reduce_scatter | solution.py:79
  513.3 20.4 %copy-start.1 = (bf16[256,2048]{1,0:T(8,128)(2,1)S(1)}, bf16[256,2048]{1,0:T(8,128)(2,1)}, u32[]{:S(2)}) copy-start(bf16[256,2048]{1,0:T(8,128)(2,1)} %fusion.10) | copy-start | bytes 3145732
  538.8 84.3 %copy-start.8 = (bf16[2,176,2048]{2,1,0:T(8,128)(2,1)S(1)}, bf16[2,176,2048]{2,1,0:T(8,128)(2,1)}, u32[]{:S(2)}) copy-start(bf16[2,176,2048]{2,1,0:T(8,128)(2,1)} %all-gather.9.cloned.1.call-done) | copy-start | bytes 4325380
  623.2 1.9 copy-start.9
  625.0 1.9 copy-start.10
  626.9 1.9 copy-start.2
  628.8 1.9 copy-start.3
  630.7 1.9 copy-start.4
Sparse Core Ops, SparseCore 0:
  41.6 7.2 all-gather.8
  65.3 7.2 all-gather.10
  89.8 7.2 all-gather.12
  102.4 395.6 all-gather.20
  500.1 7.7 all-gather.14
  509.9 10.7 all-gather.16
  522.9 10.7 all-gather.18
  539.0 82.5 reduce-scatter.1
